TPU v7x, 512 devices: a whole 4x8x8 slice. The times are simulated.
512 devices in a mesh: sp: 64 (over z, y), fs: 4 (over x), tp: 2 (over core).
Axes of the slice: x: 4, y: 8, z: 8, core: 2. Of those that a mesh axis runs over, the one named last changes fastest.
Arguments:
- tokens: bfloat16 [32768, 2048], P(('fs', 'sp')), may hold values from -6 to 6
- in_gain: float32 [2048], replicated, may hold values from 0.1 to 1.9
- query_weight: bfloat16 [2048, 512], P(None, ('tp', 'fs')), may hold values from -0.17291713 to 0.17291713
- key_weight: bfloat16 [2048, 512], P(None, ('tp', 'fs')), may hold values from -0.17291713 to 0.17291713
- value_weight: bfloat16 [2048, 512], P(None, ('tp', 'fs')), may hold values from -0.125 to 0.125
- rec_query_weight: bfloat16 [2048, 512], P(None, ('tp', 'fs')), may hold values from -0.125 to 0.125
- rec_forget_weight: bfloat16 [2048, 512], P(None, ('tp', 'fs')), may hold values from -0.125 to 0.125
- rec_input_weight: bfloat16 [2048, 512], P(None, ('tp', 'fs')), may hold values from -0.125 to 0.125
- mix_lambda: float32 [4], P('tp'), may hold values from 0.3 to 0.8
- lower_bound: float32 [4, 128], P('tp'), may hold values from 0.9 to 0.9999695
- forget_scale: float32 [32768], P(('fs', 'sp')), may hold values from 0.35 to 24576
- att_gain: float32 [128], replicated, may hold values from 0.1 to 1.9
- recurrence_gain: float32 [128], replicated, may hold values from 0.1 to 1.9
- att_out_weight: bfloat16 [512, 2048], P('tp'), may hold values from -0.1875 to 0.1875
- rec_out_weight: bfloat16 [512, 2048], P('tp'), may hold values from -0.1875 to 0.1875
Outputs:
- mixed_out: bfloat16 [32768, 2048], P(('fs', 'sp'))
- log_weight_sum: float32 [4, 32768], P('tp', ('fs', 'sp'))
All inputs are finite; a program needn't handle non-finite values.
Results may differ from a plain program's by a relative error of at most 0.012.
Values may be sent and summed in bfloat16 or wider, within the bound.
A program may use at most 128 MiB of HBM per device.

v0:
```python
import functools

import jax
import jax.numpy as jnp
from jax import lax
from jax.experimental import pallas as pl
from jax.experimental.pallas import tpu as pltpu
from jax.sharding import PartitionSpec as P

DK = 64
DV = 128
SUB = 16
EPS = 1e-06
NEG = -1e30
MESH = pl.DeviceIdType.MESH


def dot_nt(a, b):
    return lax.dot_general(a, b, (((1,), (1,)), ((), ())), preferred_element_type=jnp.float32)


def dot_nn(a, b):
    return jnp.dot(a, b, preferred_element_type=jnp.float32)


def partner(f, d, n, sign):
    if n & (n - 1):
        return lax.rem(f + sign * d + n, n)
    out, bit = 0, 1
    while bit < n:
        mine = lax.rem(f // bit, 2)
        out = out + bit * ((1 - mine) if d & bit else mine)
        bit *= 2
    return out


def kernel(
    n_sp, n_fs, n_tp, st_dtype,
    tok, gain, w0, w1, w2, w3, w4, w5, lam, lower, scale, att_gain, rec_gain, aow, row_w,
    parts, lse,
    aov, rov, wcat, tok_all, nrm, psend, osend, kvall, pr,
    smat, olocal, qdec, send_st, s_in, s_out, m_s, l_s, acc,
    w_sem, o_sem, tok_s, tok_r, rel_s, rel_r, a_s, a_r, b_s, b_r, kv_s, kv_r, st_s, st_r, op_s, op_r,
):
    z, f, t = lax.axis_index("sp"), lax.axis_index("fs"), lax.axis_index("tp")
    rows, width = tok.shape
    half = rows // n_tp
    heads = n_fs // 2
    nxt, prv = lax.rem(z + 1, n_sp), lax.rem(z + n_sp - 1, n_sp)

    order = (2, 0, 1, 3, 4, 5)
    wcopies = [
        pltpu.make_async_copy(w, wcat.at[pl.ds(order[i] * DK, DK)], w_sem.at[i])
        for i, w in enumerate((w0, w1, w2, w3, w4, w5))
    ]
    for c in wcopies:
        c.start()
    ocopies = [
        pltpu.make_async_copy(aow, aov, o_sem.at[0]),
        pltpu.make_async_copy(row_w, rov, o_sem.at[1]),
    ]

    barrier = pltpu.get_barrier_semaphore()
    for d in range(1, n_fs):
        pl.semaphore_signal(barrier, inc=1, device_id={"fs": partner(f, d, n_fs, 1)}, device_id_type=MESH)
    for d in range(1, n_tp):
        pl.semaphore_signal(barrier, inc=1, device_id={"tp": lax.rem(t + d, n_tp)}, device_id_type=MESH)
    pl.semaphore_signal(barrier, inc=1, device_id={"sp": nxt}, device_id_type=MESH)
    pl.semaphore_signal(barrier, inc=1, device_id={"sp": prv}, device_id_type=MESH)
    pl.semaphore_wait(barrier, n_fs - 1 + n_tp - 1 + 2)

    my_half = pl.ds(pl.multiple_of(t * half, half), half)
    tok_copies = []
    for d in range(1, n_fs):
        c = pltpu.make_async_remote_copy(
            tok.at[my_half], tok_all.at[d - 1, my_half], tok_s.at[d - 1], tok_r.at[d - 1],
            device_id={"fs": partner(f, d, n_fs, 1)}, device_id_type=MESH,
        )
        c.start()
        tok_copies.append(c)
    for c in ocopies:
        c.start()

    for c in wcopies:
        c.wait()

    blk = 32

    def project(src_ref):
        @pl.loop(0, rows // blk)
        def _(i):
            sl = pl.ds(pl.multiple_of(i * blk, blk), blk)
            x = src_ref[sl, :].astype(jnp.float32)
            ms = jnp.mean(x * x, axis=-1, keepdims=True)
            nrm[sl, :] = (x * lax.rsqrt(ms + EPS) * gain[...]).astype(jnp.bfloat16)

        return dot_nt(nrm[...], wcat[...]).astype(jnp.bfloat16)

    own = project(tok)
    kvall[z, f] = own[:, : 2 * DK]
    pr[f, 0] = own[:, 2 * DK: 4 * DK]
    pr[f, 1] = own[:, 4 * DK:]

    relays = {}
    for d in range(1, n_fs):
        tok_copies[d - 1].wait_recv()
        for e in range(1, n_tp):
            c = pltpu.make_async_remote_copy(
                tok_all.at[d - 1, my_half], tok_all.at[d - 1, my_half],
                rel_s.at[d - 1, e - 1], rel_r.at[d - 1, e - 1],
                device_id={"tp": lax.rem(t + e, n_tp)}, device_id_type=MESH,
            )
            c.start()
            relays[d, e] = c
        for e in range(1, n_tp):
            relays[d, e].wait_recv()
        got = project(tok_all.at[d - 1])
        to = partner(f, d, n_fs, -1)
        psend[d - 1] = got[:, : 2 * DK]
        osend[d - 1, 0] = got[:, 2 * DK: 4 * DK]
        osend[d - 1, 1] = got[:, 4 * DK:]
        ca = pltpu.make_async_remote_copy(
            psend.at[d - 1], kvall.at[z, f], a_s.at[d - 1], a_r.at[d - 1],
            device_id={"fs": to}, device_id_type=MESH,
        )
        ca.start()
        cb = pltpu.make_async_remote_copy(
            osend.at[d - 1], pr.at[f], b_s.at[d - 1], b_r.at[d - 1],
            device_id={"fs": to}, device_id_type=MESH,
        )
        cb.start()
        relays[d, "a"] = ca
        relays[d, "b"] = cb

    def forward(c, p):
        return pltpu.make_async_remote_copy(
            kvall.at[c, p], kvall.at[c, p], kv_s.at[c, p], kv_r.at[c, p],
            device_id={"sp": nxt}, device_id_type=MESH,
        )

    has_next = z + 1 < n_sp
    for d in range(n_fs):
        if d:
            relays[d, "a"].wait_recv()
        p = partner(f, d, n_fs, 1)

        @pl.when(has_next)
        def _():
            forward(z, p).start()

    for d in range(1, n_fs):
        relays[d, "b"].wait_recv()

    ri_row = lax.broadcasted_iota(jnp.int32, (rows, DV), 0)
    sub_pos = lax.rem(ri_row, SUB)
    tri = (
        lax.broadcasted_iota(jnp.int32, (rows, rows), 0)
        >= lax.broadcasted_iota(jnp.int32, (rows, rows), 1)
    )
    trif = tri.astype(jnp.float32)
    sc = jnp.broadcast_to(scale[...], (DV, rows)).T
    tails = []
    gates = []
    for h in range(heads):
        rf = jnp.concatenate([pr[2 * h, 1, :, :DK], pr[2 * h + 1, 1, :, :DK]], axis=1).astype(jnp.float32)
        ri = jnp.concatenate([pr[2 * h, 1, :, DK:], pr[2 * h + 1, 1, :, DK:]], axis=1).astype(jnp.float32)
        lb = lower[h: h + 1, :]
        g = sc * jnp.log(lb + (1.0 - lb) * jax.nn.sigmoid(rf))
        kk = 1.0 - jnp.exp(g)
        a = jnp.dot(trif, g, preferred_element_type=jnp.float32, precision=lax.Precision.HIGHEST)
        last = a[rows - 1: rows, :]
        kd = (kk * jnp.exp(last - a)).astype(jnp.bfloat16)
        s_out[h] = dot_nn(ri.T.astype(jnp.bfloat16), kd)
        tails.append(jnp.exp(last))
        gates.append((a, kk, ri))

    def send_state():
        return pltpu.make_async_remote_copy(
            send_st, s_in, st_s, st_r, device_id={"sp": nxt}, device_id_type=MESH
        )

    @pl.when((z == 0) & has_next)
    def _():
        send_st[...] = s_out[...].astype(st_dtype)
        send_state().start()

    def attend(c, first):
        for h in range(heads):
            vh = jnp.concatenate([kvall[c, 2 * h, :, DK:], kvall[c, 2 * h + 1, :, DK:]], axis=1)
            for m in range(2):
                i = 2 * h + m
                sco = dot_nt(pr[i, 0, :, :DK], kvall[c, i, :, :DK]) * DK ** (-0.5)
                if first:
                    sco = jnp.where(tri, sco, NEG)
                    top = jnp.max(sco, axis=-1, keepdims=True)
                    e = jnp.exp(sco - top)
                    l_s[i] = jnp.sum(e, axis=-1, keepdims=True)
                    acc[i] = dot_nn(e.astype(jnp.bfloat16), vh)
                    m_s[i] = top
                else:
                    old = m_s[i]
                    top = jnp.maximum(old, jnp.max(sco, axis=-1, keepdims=True))
                    e = jnp.exp(sco - top)
                    shrink = jnp.exp(old - top)
                    l_s[i] = l_s[i] * shrink + jnp.sum(e, axis=-1, keepdims=True)
                    acc[i] = acc[i] * shrink + dot_nn(e.astype(jnp.bfloat16), vh)
                    m_s[i] = top

    attend(z, True)

    for h in range(heads):
        a, kk, ri = gates[h]
        rq = jnp.concatenate([pr[2 * h, 0, :, DK:], pr[2 * h + 1, 0, :, DK:]], axis=1).astype(jnp.float32)
        qdec[h] = (rq * jnp.exp(a)).astype(jnp.bfloat16)
        smat[h, 0:SUB, :] = jnp.zeros((SUB, rows), jnp.bfloat16)
        for i in range(1, rows // SUB):
            lo = i * SUB
            ref = a[lo - 1: lo, :]
            qd = (rq[lo: lo + SUB] * jnp.exp(a[lo: lo + SUB] - ref)).astype(jnp.bfloat16)
            kd = (kk * jnp.exp(jnp.where(ri_row < lo, ref - a, NEG))).astype(jnp.bfloat16)
            smat[h, lo: lo + SUB, :] = dot_nt(qd, kd).astype(jnp.bfloat16)
        o = dot_nn(smat[h], ri.astype(jnp.bfloat16))
        o = o + jnp.sum(rq * kk, axis=-1, keepdims=True) * ri
        for d in range(1, SUB):
            valid = sub_pos >= d
            dec = jnp.exp(jnp.where(valid, a - pltpu.roll(a, d, 0), NEG))
            col = jnp.sum(rq * dec * pltpu.roll(kk, d, 0), axis=-1, keepdims=True)
            o = o + col * pltpu.roll(ri, d, 0)
        olocal[h] = o

    @pl.loop(0, z)
    def _(s):
        c = z - 1 - s
        for p in range(n_fs):
            cp = forward(c, p)
            cp.wait_recv()

            @pl.when(has_next)
            def _():
                cp.start()

        attend(c, False)

    @pl.when(z > 0)
    def _():
        send_state().wait_recv()

    @pl.when((z > 0) & has_next)
    def _():
        for h in range(heads):
            send_st[h] = (tails[h] * s_in[h].astype(jnp.float32) + s_out[h]).astype(st_dtype)
        send_state().start()

    @pl.when(z > 0)
    def _():
        for h in range(heads):
            olocal[h] = olocal[h] + dot_nt(qdec[h], s_in[h].astype(jnp.bfloat16))

    atts, recs = [], []
    ag, rg = att_gain[...], rec_gain[...]
    lane = lax.broadcasted_iota(jnp.int32, (rows, DV), 1)
    lses = jnp.zeros((rows, DV), jnp.float32)
    for h in range(heads):
        x = acc[2 * h] / l_s[2 * h] - lam[0, h] * (acc[2 * h + 1] / l_s[2 * h + 1])
        ms = jnp.mean(x * x, axis=-1, keepdims=True)
        atts.append((x * lax.rsqrt(ms + EPS) * ag * 0.8).astype(jnp.bfloat16))
        o = olocal[h]
        ms = jnp.mean(o * o, axis=-1, keepdims=True)
        recs.append((o * lax.rsqrt(ms + EPS) * rg).astype(jnp.bfloat16))
        lses = jnp.where(lane == h, m_s[2 * h] + jnp.log(l_s[2 * h]), lses)
    lse[...] = lses.T[:heads, :]
    att = jnp.concatenate(atts, axis=1)
    rec = jnp.concatenate(recs, axis=1)
    for c in ocopies:
        c.wait()
    pieces = 4
    cols = width // pieces
    swaps = []
    for j in range(pieces):
        sl = slice(j * cols, (j + 1) * cols)
        parts[0, :, sl] = (dot_nn(att, aov[:, sl]) + dot_nn(rec, rov[:, sl])).astype(jnp.bfloat16)
        for e in range(1, n_tp):
            c = pltpu.make_async_remote_copy(
                parts.at[0, :, sl], parts.at[e, :, sl], op_s.at[e - 1, j], op_r.at[e - 1, j],
                device_id={"tp": lax.rem(t + e, n_tp)}, device_id_type=MESH,
            )
            c.start()
            swaps.append(c)

    for c in tok_copies:
        c.wait_send()
    for d in range(1, n_fs):
        for e in range(1, n_tp):
            relays[d, e].wait_send()
        relays[d, "a"].wait_send()
        relays[d, "b"].wait_send()
    @pl.when(has_next)
    def _():
        send_state().wait_send()

        @pl.loop(0, z + 1)
        def _(c):
            for p in range(n_fs):
                forward(c, p).wait_send()

    for c in swaps:
        c.wait()


def finish(parts, lse_in, mixed, lse):
    total = parts[0].astype(jnp.float32)
    for e in range(1, parts.shape[0]):
        total = total + parts[e].astype(jnp.float32)
    mixed[...] = total.astype(jnp.bfloat16)
    lse[...] = lse_in[...]


def solution(mesh):
    n_sp, n_fs, n_tp = (mesh.shape[k] for k in ("sp", "fs", "tp"))
    st_dtype = jnp.bfloat16 if n_sp <= 8 else jnp.float32

    def on_device(
        tokens, in_gain, wq, wk, wvv, wrq, wrf, wri, lam, lower, scale, att_gain, rec_gain, aow, row_w
    ):
        rows, width = tokens.shape
        heads = lower.shape[0]
        assert heads * 2 == n_fs and rows % (8 * n_tp) == 0
        vm = pl.BlockSpec(memory_space=pltpu.VMEM)
        sm = pl.BlockSpec(memory_space=pltpu.SMEM)
        hbm = pl.BlockSpec(memory_space=pl.ANY)
        bf, f32 = jnp.bfloat16, jnp.float32
        dma = pltpu.SemaphoreType.DMA
        peers = n_fs - 1
        pieces = 4
        parts, lse = pl.pallas_call(
            functools.partial(kernel, n_sp, n_fs, n_tp, st_dtype),
            out_shape=(
                jax.ShapeDtypeStruct((n_tp, rows, width), bf),
                jax.ShapeDtypeStruct((heads, rows), f32),
            ),
            in_specs=[vm, vm] + [hbm] * 6 + [sm, vm, vm, vm, vm, hbm, hbm],
            out_specs=(vm, vm),
            scratch_shapes=[
                pltpu.VMEM(aow.shape, bf),
                pltpu.VMEM(row_w.shape, bf),
                pltpu.VMEM((6 * DK, width), bf),
                pltpu.VMEM((peers, rows, width), bf),
                pltpu.VMEM((rows, width), bf),
                pltpu.VMEM((peers, rows, 2 * DK), bf),
                pltpu.VMEM((peers, 2, rows, 2 * DK), bf),
                pltpu.VMEM((n_sp, n_fs, rows, 2 * DK), bf),
                pltpu.VMEM((n_fs, 2, rows, 2 * DK), bf),
                pltpu.VMEM((heads, rows, rows), bf),
                pltpu.VMEM((heads, rows, DV), f32),
                pltpu.VMEM((heads, rows, DV), bf),
                pltpu.VMEM((heads, DV, DV), st_dtype),
                pltpu.VMEM((heads, DV, DV), st_dtype),
                pltpu.VMEM((heads, DV, DV), f32),
                pltpu.VMEM((2 * heads, rows, 1), f32),
                pltpu.VMEM((2 * heads, rows, 1), f32),
                pltpu.VMEM((2 * heads, rows, DV), f32),
                dma((6,)), dma((2,)),
                dma((peers,)), dma((peers,)),
                dma((peers, n_tp - 1)), dma((peers, n_tp - 1)),
                dma((peers,)), dma((peers,)), dma((peers,)), dma((peers,)),
                dma((n_sp, n_fs)), dma((n_sp, n_fs)),
                dma, dma,
                dma((n_tp - 1, pieces)), dma((n_tp - 1, pieces)),
            ],
            compiler_params=pltpu.CompilerParams(
                collective_id=0, has_side_effects=True, vmem_limit_bytes=56 * 1024 * 1024
            ),
            name="mixer",
        )(
            tokens, in_gain[None], wq.T, wk.T, wvv.T, wrq.T, wrf.T, wri.T, lam[None], lower, scale[None],
            att_gain[None], rec_gain[None], aow, row_w,
        )
        half = width // 2
        return pl.pallas_call(
            finish,
            grid=(2,),
            out_shape=(
                jax.ShapeDtypeStruct((rows, width), bf),
                jax.ShapeDtypeStruct((heads, rows), f32),
            ),
            in_specs=[
                pl.BlockSpec((n_tp, rows, half), lambda i: (0, 0, i)),
                pl.BlockSpec((heads, rows), lambda i: (0, 0)),
            ],
            out_specs=(
                pl.BlockSpec((rows, half), lambda i: (0, i)),
                pl.BlockSpec((heads, rows), lambda i: (0, 0)),
            ),
            name="finish",
        )(parts, lse)

    col = P(None, ("tp", "fs"))
    return jax.shard_map(
        on_device,
        mesh=mesh,
        in_specs=(
            P(("fs", "sp"), None), P(), col, col, col, col, col, col,
            P("tp"), P("tp", None), P(("fs", "sp")), P(), P(), P("tp", None), P("tp", None),
        ),
        out_specs=(P(("fs", "sp"), None), P("tp", ("fs", "sp"))),
        check_vma=False,
    )
```

profile of v0, /device:TPU:505, one launch (start us, length us, event | category | flops | bytes accessed | tf_op | source)
XLA Modules:
  0.0 303.6 jit_solution(8807016634463855171)
XLA Ops:
  0.6 301.0 %mixer.1 = (bf16[2,128,2048]{2,1,0:T(8,128)(2,1)}, f32[2,128]{1,0:T(2,128)}) custom-call(bf16[128,2048]{1,0:T(8,128)(2,1)} %tok.1, f32[1,2048]{1,0:T(1,128)} %bitcast.17, bf16[64,2048]{1,0:T(8,128)(2,1)} %bitcast.11, bf16[64,2048]{1,0:T(8,128)(2,1)} %bitcast.12, bf16[64,2048]{1,0:T(8,128)(2,1)} %bitcast.13, bf16[64,2048]{1,0:T(8,128)(2,1)} %bitcast.14, ...), custom_call_target="tpu_custom_call" | custom-call | tf_op jit(solution)/shard_map/mixer/pallas_call | solution.py:335
  301.6 2.0 finish.1
where the time goes:
time: 304 us
  Pallas kernels  303 us (100%)
    pallas_call x1, Pallas kernels, on_device(): pl.pallas_call(functools.partial(kernel, n_sp, n_fs, n_tp, st_dtype), out...  301 us

commit v1 on v0

v1 whole, which is shorter than its diff:
```python
import functools

import jax
import jax.numpy as jnp
from jax import lax
from jax.experimental import pallas as pl
from jax.experimental.pallas import tpu as pltpu
from jax.sharding import PartitionSpec as P

DK = 64
DV = 128
SUB = 16
EPS = 1e-06
NEG = -1e30
MESH = pl.DeviceIdType.MESH
BF = jnp.bfloat16
F32 = jnp.float32


def dot_nt(a, b):
    return lax.dot_general(a, b, (((1,), (1,)), ((), ())), preferred_element_type=jnp.float32)


def dot_nn(a, b):
    return jnp.dot(a, b, preferred_element_type=jnp.float32)


def grid_of(n_sp):
    ny = 1
    while ny * ny < n_sp:
        ny *= 2
    return n_sp // ny, ny


def kernel(
    n_sp, n_fs, n_tp,
    tok, gain, w0, w1, w2, w3, w4, w5, lam, lower, scale, att_gain, rec_gain, aow, row_w,
    parts, lse,
    aov, rov, wcat, nall, psend, pr, q2, kv2, kvg, qb, osnd, ssnd, orcv, srcv, m_s, l_s, acc,
    smat, olocal, qdec, lsend, lrec, tl, trec, pre, tsnd, rdsnd, zrec, zrd, r3s, s_in,
    w_sem, o_sem, x_s, x_r, f_s, f_r, rel_s, rel_r, b_s, b_r, fo_s, fo_r, kv_s, kv_r, q_s, q_r,
    os_s, os_r, ss_s, ss_r, r1_s, r1_r, r1t_s, r1t_r, r2_s, r2_r, r2t_s, r2t_r, r3_s, r3_r, op_s, op_r,
):
    nz, ny = grid_of(n_sp)
    hz = nz // 2
    sl_rows = DV // ny
    z, f, t = lax.axis_index("sp"), lax.axis_index("fs"), lax.axis_index("tp")
    i, j = z // ny, lax.rem(z, ny)
    mir = nz - 1 - i
    low = jnp.minimum(i, mir)
    hd = jnp.where(i < hz, 0, 1)
    rows, width = tok.shape
    half = rows // n_tp
    quart = half // 2
    heads = n_fs // 2
    right, left = lax.rem(f + 1, n_fs), lax.rem(f + n_fs - 1, n_fs)
    across = lax.rem(f + 2, n_fs)
    j_r, j_l = lax.rem(j + 1, ny), lax.rem(j + ny - 1, ny)

    def remote(src, dst, s, r, **dev):
        return pltpu.make_async_remote_copy(src, dst, s, r, device_id=dev, device_id_type=MESH)

    def sp_of(a, b):
        return a * ny + b

    wcopies = [
        pltpu.make_async_copy(w, wcat.at[pl.ds(n * DK, DK)], w_sem.at[n])
        for n, w in enumerate((w0, w1, w2, w3, w4, w5))
    ]
    for c in wcopies:
        c.start()
    ocopies = [
        pltpu.make_async_copy(aow, aov, o_sem.at[0]),
        pltpu.make_async_copy(row_w, rov, o_sem.at[1]),
    ]

    barrier = pltpu.get_barrier_semaphore()
    for d in range(1, n_fs):
        pl.semaphore_signal(barrier, inc=1, device_id={"fs": lax.rem(f + d, n_fs)}, device_id_type=MESH)
    for d in range(1, n_tp):
        pl.semaphore_signal(barrier, inc=1, device_id={"tp": lax.rem(t + d, n_tp)}, device_id_type=MESH)
    for d in range(1, ny):
        pl.semaphore_signal(barrier, inc=1, device_id={"sp": sp_of(i, lax.rem(j + d, ny))}, device_id_type=MESH)
    for d in range(1, nz):
        pl.semaphore_signal(barrier, inc=1, device_id={"sp": sp_of(lax.rem(i + d, nz), j)}, device_id_type=MESH)

    blk = 32

    @pl.loop(0, rows // blk)
    def _(n):
        sl = pl.ds(pl.multiple_of(n * blk, blk), blk)
        x = tok[sl, :].astype(F32)
        ms = jnp.mean(x * x, axis=-1, keepdims=True)
        nall[0, sl, :] = (x * lax.rsqrt(ms + EPS) * gain[...]).astype(BF)

    st_row = lax.broadcasted_iota(jnp.int32, (8, DV), 0)
    for k in range(1, hz):
        @pl.when(k > i)
        def _():
            for a in (k, nz - 1 - k):
                orcv[a] = jnp.zeros((2, rows, DV), BF)
                srcv[a] = jnp.where(st_row < 2, NEG, 0.0)
    for a in range(nz):
        @pl.when(i <= a)
        def _():
            zrec[a] = jnp.zeros((heads, sl_rows, DV), BF)
            zrd[a] = jnp.ones((heads, DV), F32)

    pl.semaphore_wait(barrier, n_fs - 1 + n_tp - 1 + ny - 1 + nz - 1)

    def pc(n):
        return pl.ds(pl.multiple_of(t * half + n * quart, quart), quart)

    x_a = remote(nall.at[0, pc(0)], nall.at[1, pc(0)], x_s.at[0], x_r.at[0], fs=right)
    x_b = remote(nall.at[0, pc(1)], nall.at[2, pc(1)], x_s.at[1], x_r.at[1], fs=left)
    x_c = remote(nall.at[0, pc(1)], nall.at[1, pc(1)], x_s.at[2], x_r.at[2], fs=right)
    x_d = remote(nall.at[0, pc(0)], nall.at[2, pc(0)], x_s.at[3], x_r.at[3], fs=left)
    f_a = remote(nall.at[1, pc(0)], nall.at[3, pc(0)], f_s.at[0], f_r.at[0], fs=right)
    f_b = remote(nall.at[2, pc(1)], nall.at[3, pc(1)], f_s.at[1], f_r.at[1], fs=left)
    for c in (x_a, x_b, x_c, x_d):
        c.start()
    for c in ocopies:
        c.start()

    relays = []

    def relay(slot, n, idx):
        for e in range(1, n_tp):
            c = remote(
                nall.at[slot, pc(n)], nall.at[slot, pc(n)], rel_s.at[e - 1, idx], rel_r.at[e - 1, idx],
                tp=lax.rem(t + e, n_tp),
            )
            c.start()
            relays.append(c)

    def relay_wait(slot, n, idx):
        for e in range(1, n_tp):
            oth = lax.rem(t + n_tp - e, n_tp)
            sl = pl.ds(pl.multiple_of(oth * half + n * quart, quart), quart)
            remote(
                nall.at[slot, sl], nall.at[slot, sl], rel_s.at[e - 1, idx], rel_r.at[e - 1, idx],
                tp=lax.rem(t + e, n_tp),
            ).wait_recv()

    def project(slot):
        return dot_nt(nall[slot], wcat[...]).astype(BF)

    for c in wcopies:
        c.wait()
    own = project(0)
    for g in range(3):
        pr[f, g] = own[:, g * DV: (g + 1) * DV]

    x_a.wait_recv()
    f_a.start()
    relay(1, 0, 0)
    x_b.wait_recv()
    f_b.start()
    relay(2, 1, 1)
    x_c.wait_recv()
    relay(1, 1, 2)
    x_d.wait_recv()
    relay(2, 0, 3)

    back = (left, right, across)
    res = [
        remote(psend.at[n], pr.at[f], b_s.at[n], b_r.at[n], fs=back[n]) for n in range(3)
    ]

    def deliver(slot):
        got = project(slot)
        for g in range(3):
            psend[slot - 1, g] = got[:, g * DV: (g + 1) * DV]
        res[slot - 1].start()

    relay_wait(1, 0, 0)
    relay_wait(1, 1, 2)
    deliver(1)
    relay_wait(2, 1, 1)
    relay_wait(2, 0, 3)
    deliver(2)
    f_a.wait_recv()
    relay(3, 0, 4)
    f_b.wait_recv()
    relay(3, 1, 5)
    relay_wait(3, 0, 4)
    relay_wait(3, 1, 5)
    deliver(3)

    came = (right, left, across)
    for n in range(3):
        remote(psend.at[n], pr.at[came[n]], b_s.at[n], b_r.at[n], fs=back[n]).wait_recv()

    def pair(h, g, lo):
        return jnp.concatenate([pr[2 * h, g, :, lo: lo + DK], pr[2 * h + 1, g, :, lo: lo + DK]], axis=1)

    for h in range(heads):
        kv2[h, :, :DV] = pair(h, 0, DK)
        kv2[h, :, DV:] = pair(h, 1, 0)
        q2[h] = (pair(h, 0, 0).astype(F32) * DK ** (-0.5)).astype(BF)

    fold = remote(kv2.at[1 - hd], kvg.at[1, j], fo_s, fo_r, sp=sp_of(mir, j))
    fold.start()
    kvg[0, j] = kv2[hd]
    qb[i] = q2[hd]

    right_hops = (ny // 2, ny - 1 - ny // 2)
    left_hops = (ny - 1 - ny // 2, ny // 2)

    def ring(g, way, d):
        y = lax.rem(j + (d if way else ny - d), ny)
        return remote(
            kvg.at[g, y], kvg.at[g, y], kv_s.at[g, way, d], kv_r.at[g, way, d],
            sp=sp_of(i, j_l if way else j_r),
        )

    def ring_wait(g, way, d):
        y = lax.rem(j + (d + 1 if way else ny - d - 1), ny)
        remote(
            kvg.at[g, y], kvg.at[g, y], kv_s.at[g, way, d], kv_r.at[g, way, d],
            sp=sp_of(i, j_l if way else j_r),
        ).wait_recv()

    hops = [(right_hops[g], left_hops[g]) for g in range(2)]

    def step(g, d):
        for way in range(2):
            if 0 < d <= hops[g][way]:
                ring_wait(g, way, d - 1)
            if d < hops[g][way]:
                ring(g, way, d).start()

    step(0, 0)

    def q_copy(a):
        return remote(q2.at[0 if a < hz else 1], qb.at[i], q_s.at[a], q_r.at[i], sp=sp_of(a, j))

    def wanted(a):
        return (min(a, nz - 1 - a) <= i) & (i != a)

    for a in range(nz):
        @pl.when(wanted(a))
        def _():
            q_copy(a).start()

    ri_row = lax.broadcasted_iota(jnp.int32, (rows, DV), 0)
    lane = lax.broadcasted_iota(jnp.int32, (rows, DV), 1)
    sub_pos = lax.rem(ri_row, SUB)
    tri = (
        lax.broadcasted_iota(jnp.int32, (rows, rows), 0)
        >= lax.broadcasted_iota(jnp.int32, (rows, rows), 1)
    )
    trif = tri.astype(F32)
    sc = jnp.broadcast_to(scale[...], (DV, rows)).T
    gates = []
    for h in range(heads):
        rf = pair(h, 2, 0).astype(F32)
        ri = pair(h, 2, DK).astype(F32)
        lb = lower[h: h + 1, :]
        g = sc * jnp.log(lb + (1.0 - lb) * jax.nn.sigmoid(rf))
        kk = 1.0 - jnp.exp(g)
        a = jnp.dot(trif, g, preferred_element_type=F32, precision=lax.Precision.HIGHEST)
        last = a[rows - 1: rows, :]
        kd = (kk * jnp.exp(last - a)).astype(BF)
        lsend[h] = dot_nn(ri.T.astype(BF), kd).astype(BF)
        tl[h: h + 1, :] = jnp.exp(last)
        gates.append((a, kk, ri))

    def sl_of(y):
        return pl.ds(pl.multiple_of(y * sl_rows, sl_rows), sl_rows)

    def r1(d):
        y = lax.rem(j + d, ny)
        return (
            remote(lsend.at[:, sl_of(y)], lrec.at[j], r1_s.at[d], r1_r.at[d], sp=sp_of(i, y)),
            remote(tl, trec.at[j], r1t_s.at[d], r1t_r.at[d], sp=sp_of(i, y)),
        )

    def r1_wait(d):
        y = lax.rem(j + ny - d, ny)
        to = sp_of(i, lax.rem(j + d, ny))
        remote(lsend.at[:, sl_of(j)], lrec.at[y], r1_s.at[d], r1_r.at[d], sp=to).wait_recv()
        remote(tl, trec.at[y], r1t_s.at[d], r1t_r.at[d], sp=to).wait_recv()

    lrec[j] = lsend[:, sl_of(j), :]
    trec[j] = tl[...]
    for d in range(1, ny):
        for c in r1(d):
            c.start()

    fold.wait_recv()
    step(1, 0)
    step(0, 1)

    def local(h):
        a, kk, ri = gates[h]
        rq = pair(h, 1, DK).astype(F32)
        qdec[h] = (rq * jnp.exp(a)).astype(BF)
        smat[h, 0:SUB, :] = jnp.zeros((SUB, rows), BF)
        for n in range(1, rows // SUB):
            lo = n * SUB
            ref = a[lo - 1: lo, :]
            qd = (rq[lo: lo + SUB] * jnp.exp(a[lo: lo + SUB] - ref)).astype(BF)
            kd = (kk * jnp.exp(jnp.where(ri_row < lo, ref - a, NEG))).astype(BF)
            smat[h, lo: lo + SUB, :] = dot_nt(qd, kd).astype(BF)
        o = dot_nn(smat[h], ri.astype(BF))
        o = o + jnp.sum(rq * kk, axis=-1, keepdims=True) * ri
        for d in range(1, SUB):
            valid = sub_pos >= d
            dec = jnp.exp(jnp.where(valid, a - pltpu.roll(a, d, 0), NEG))
            col = jnp.sum(rq * dec * pltpu.roll(kk, d, 0), axis=-1, keepdims=True)
            o = o + col * pltpu.roll(ri, d, 0)
        olocal[h] = o

    local(0)
    step(1, 1)
    step(0, 2)

    for d in range(1, ny):
        r1_wait(d)
    run = jnp.zeros((heads, sl_rows, DV), F32)
    rd = jnp.ones((heads, DV), F32)
    for y in range(ny):
        pre[y] = run
        run = trec[y][:, None, :] * run + lrec[y].astype(F32)
        rd = rd * trec[y]
    tsnd[...] = run.astype(BF)
    rdsnd[...] = rd

    def r2(a):
        return (
            remote(tsnd, zrec.at[i], r2_s.at[a], r2_r.at[i], sp=sp_of(a, j)),
            remote(rdsnd, zrd.at[i], r2t_s.at[a], r2t_r.at[i], sp=sp_of(a, j)),
        )

    def r2_wait(a):
        to = sp_of(lax.rem(i + 1, nz), j)
        remote(tsnd, zrec.at[a], r2_s.at[a], r2_r.at[a], sp=to).wait_recv()
        remote(rdsnd, zrd.at[a], r2t_s.at[a], r2t_r.at[a], sp=to).wait_recv()

    for a in range(1, nz):
        @pl.when(a > i)
        def _():
            for c in r2(a):
                c.start()

    local(1)
    for d in range(1, ny // 2 + 1):
        if d > 1:
            step(1, d)
        if d > 2:
            step(0, d)

    for a in range(nz - 1):
        @pl.when(a < i)
        def _():
            r2_wait(a)
    run = jnp.zeros((heads, sl_rows, DV), F32)
    for a in range(nz - 1):
        run = zrd[a][:, None, :] * run + zrec[a].astype(F32)
    for y in range(ny):
        r3s[y] = (run + pre[y]).astype(BF)
        run = trec[y][:, None, :] * run

    def r3(d):
        y = lax.rem(j + d, ny)
        return remote(r3s.at[y], s_in.at[:, sl_of(j)], r3_s.at[d], r3_r.at[d], sp=sp_of(i, y))

    def r3_wait(d):
        y = lax.rem(j + ny - d, ny)
        to = sp_of(i, lax.rem(j + d, ny))
        remote(r3s.at[y], s_in.at[:, sl_of(y)], r3_s.at[d], r3_r.at[d], sp=to).wait_recv()

    s_in[:, sl_of(j), :] = r3s[j]
    for d in range(1, ny):
        r3(d).start()

    for a in range(nz):
        @pl.when((a >= low) & (i != a))
        def _():
            remote(q2.at[0], qb.at[a], q_s.at[a], q_r.at[a], sp=sp_of(lax.rem(i + 1, nz), j)).wait_recv()

    keys = ny * rows
    off = (
        lax.broadcasted_iota(jnp.int32, (rows, keys), 1)
        - lax.broadcasted_iota(jnp.int32, (rows, keys), 0)
    )

    def strip(b, g, masked):
        q = qb[b]
        kt = kvg[g, :, :, :DV].reshape(keys, DV)
        vt = kvg[g, :, :, DV:].reshape(keys, DV)
        for m in range(2):
            qm = jnp.where((lane < DK) if m == 0 else (lane >= DK), q, jnp.zeros_like(q))
            sco = dot_nt(qm, kt)
            if masked:
                sco = jnp.where(off <= j * rows, sco, NEG)
            old = m_s[m]
            top = jnp.maximum(old, jnp.max(sco, axis=-1, keepdims=True))
            e = jnp.exp(sco - top)
            shrink = jnp.exp(old - top)
            l_s[m] = l_s[m] * shrink + jnp.sum(e, axis=-1, keepdims=True)
            acc[m] = acc[m] * shrink + dot_nn(e.astype(BF), vt)
            m_s[m] = top

    def out_copies(b):
        to = sp_of(b, j)
        return (
            remote(osnd.at[b], orcv.at[i], os_s.at[b], os_r.at[i], sp=to),
            remote(ssnd.at[b], srcv.at[i], ss_s.at[b], ss_r.at[i], sp=to),
        )

    @pl.loop(0, nz - low)
    def _(n):
        b = nz - 1 - n
        m_s[...] = jnp.full(m_s.shape, NEG, F32)
        l_s[...] = jnp.zeros(l_s.shape, F32)
        acc[...] = jnp.zeros(acc.shape, F32)

        @pl.loop(0, 2)
        def _(g):
            row = jnp.where(g == 0, i, mir)

            @pl.when(b == row)
            def _():
                strip(b, g, True)

            @pl.when(b > row)
            def _():
                strip(b, g, False)

        st = jnp.zeros((rows, DV), F32)
        for m in range(2):
            st = jnp.where(lane == m, m_s[m], st)
            st = jnp.where(lane == 2 + m, l_s[m], st)
        st = st.T[:8, :]

        @pl.when(b == i)
        def _():
            for m in range(2):
                orcv[i, m] = acc[m].astype(BF)
            srcv[i] = st

        @pl.when(b != i)
        def _():
            for m in range(2):
                osnd[b, m] = acc[m].astype(BF)
            ssnd[b] = st
            for c in out_copies(b):
                c.start()

    for d in range(1, ny):
        r3_wait(d)
    recs = []
    rg = rec_gain[...]
    for h in range(heads):
        o = olocal[h] + dot_nt(qdec[h], s_in[h])
        ms = jnp.mean(o * o, axis=-1, keepdims=True)
        recs.append((o * lax.rsqrt(ms + EPS) * rg).astype(BF))
    rec = jnp.concatenate(recs, axis=1)
    for c in ocopies:
        c.wait()

    for a in range(nz):
        @pl.when(wanted(a))
        def _():
            to = sp_of(lax.rem(i + 1, nz), j)
            remote(osnd.at[a], orcv.at[a], os_s.at[a], os_r.at[a], sp=to).wait_recv()
            remote(ssnd.at[a], srcv.at[a], ss_s.at[a], ss_r.at[a], sp=to).wait_recv()

    atts = []
    ag = att_gain[...]
    lses = jnp.zeros((rows, DV), F32)
    for h in range(heads):
        src = [k if h == 0 else nz - 1 - k for k in range(hz)]
        st = jnp.concatenate(
            [srcv[a] for a in src] + [jnp.zeros((DV - 8 * hz, DV), F32)], axis=0
        ).T
        outs = []
        for m in range(2):
            tops = [st[:, 8 * k + m: 8 * k + m + 1] for k in range(hz)]
            tots = [st[:, 8 * k + 2 + m: 8 * k + 3 + m] for k in range(hz)]
            top = tops[0]
            for x in tops[1:]:
                top = jnp.maximum(top, x)
            total = jnp.zeros((rows, 1), F32)
            num = jnp.zeros((rows, DV), F32)
            for k in range(hz):
                wk = jnp.exp(tops[k] - top)
                total = total + wk * tots[k]
                num = num + wk * orcv[src[k], m].astype(F32)
            outs.append(num / total)
            if m == 0:
                lses = jnp.where(lane == h, top + jnp.log(total), lses)
        x = outs[0] - lam[0, h] * outs[1]
        ms = jnp.mean(x * x, axis=-1, keepdims=True)
        atts.append((x * lax.rsqrt(ms + EPS) * ag * 0.8).astype(BF))
    lse[...] = lses.T[:heads, :]
    att = jnp.concatenate(atts, axis=1)

    pieces = 4
    cols = width // pieces
    swaps = []
    for n in range(pieces):
        sl = slice(n * cols, (n + 1) * cols)
        parts[0, :, sl] = (dot_nn(att, aov[:, sl]) + dot_nn(rec, rov[:, sl])).astype(BF)
        for e in range(1, n_tp):
            c = remote(
                parts.at[0, :, sl], parts.at[e, :, sl], op_s.at[e - 1, n], op_r.at[e - 1, n],
                tp=lax.rem(t + e, n_tp),
            )
            c.start()
            swaps.append(c)

    for c in (x_a, x_b, x_c, x_d, f_a, f_b, *relays, *res, fold):
        c.wait_send()
    for g in range(2):
        for way in range(2):
            for d in range(hops[g][way]):
                ring(g, way, d).wait_send()
    for d in range(1, ny):
        for c in (*r1(d), r3(d)):
            c.wait_send()
    for a in range(nz):
        @pl.when(wanted(a))
        def _():
            q_copy(a).wait_send()

        @pl.when(a > i)
        def _():
            for c in r2(a):
                c.wait_send()

        @pl.when((a >= low) & (i != a))
        def _():
            for c in out_copies(a):
                c.wait_send()
    for c in swaps:
        c.wait()


def finish(parts, lse_in, mixed, lse):
    total = parts[0].astype(jnp.float32)
    for e in range(1, parts.shape[0]):
        total = total + parts[e].astype(jnp.float32)
    mixed[...] = total.astype(jnp.bfloat16)
    lse[...] = lse_in[...]


def solution(mesh):
    n_sp, n_fs, n_tp = (mesh.shape[k] for k in ("sp", "fs", "tp"))
    nz, ny = grid_of(n_sp)

    def on_device(
        tokens, in_gain, wq, wk, wvv, wrq, wrf, wri, lam, lower, scale, att_gain, rec_gain, aow, row_w
    ):
        rows, width = tokens.shape
        heads = lower.shape[0]
        assert heads == 2 and n_fs == 4 and rows == DV and nz % 2 == 0
        vm = pl.BlockSpec(memory_space=pltpu.VMEM)
        sm = pl.BlockSpec(memory_space=pltpu.SMEM)
        hbm = pl.BlockSpec(memory_space=pl.ANY)
        dma = pltpu.SemaphoreType.DMA
        peers = n_fs - 1
        pieces = 4
        slr = DV // ny
        hmax = max(ny // 2, 1)
        parts, lse = pl.pallas_call(
            functools.partial(kernel, n_sp, n_fs, n_tp),
            out_shape=(
                jax.ShapeDtypeStruct((n_tp, rows, width), BF),
                jax.ShapeDtypeStruct((heads, rows), F32),
            ),
            in_specs=[vm, vm] + [hbm] * 6 + [sm, vm, vm, vm, vm, hbm, hbm],
            out_specs=(vm, vm),
            scratch_shapes=[
                pltpu.VMEM(aow.shape, BF),
                pltpu.VMEM(row_w.shape, BF),
                pltpu.VMEM((6 * DK, width), BF),
                pltpu.VMEM((n_fs, rows, width), BF),
                pltpu.VMEM((peers, 3, rows, DV), BF),
                pltpu.VMEM((n_fs, 3, rows, DV), BF),
                pltpu.VMEM((heads, rows, DV), BF),
                pltpu.VMEM((heads, rows, 2 * DV), BF),
                pltpu.VMEM((2, ny, rows, 2 * DV), BF),
                pltpu.VMEM((nz, rows, DV), BF),
                pltpu.VMEM((nz, 2, rows, DV), BF),
                pltpu.VMEM((nz, 8, DV), F32),
                pltpu.VMEM((nz, 2, rows, DV), BF),
                pltpu.VMEM((nz, 8, DV), F32),
                pltpu.VMEM((2, rows, 1), F32),
                pltpu.VMEM((2, rows, 1), F32),
                pltpu.VMEM((2, rows, DV), F32),
                pltpu.VMEM((heads, rows, rows), BF),
                pltpu.VMEM((heads, rows, DV), F32),
                pltpu.VMEM((heads, rows, DV), BF),
                pltpu.VMEM((heads, DV, DV), BF),
                pltpu.VMEM((ny, heads, slr, DV), BF),
                pltpu.VMEM((heads, DV), F32),
                pltpu.VMEM((ny, heads, DV), F32),
                pltpu.VMEM((ny, heads, slr, DV), F32),
                pltpu.VMEM((heads, slr, DV), BF),
                pltpu.VMEM((heads, DV), F32),
                pltpu.VMEM((nz, heads, slr, DV), BF),
                pltpu.VMEM((nz, heads, DV), F32),
                pltpu.VMEM((ny, heads, slr, DV), BF),
                pltpu.VMEM((heads, DV, DV), BF),
                dma((6,)), dma((2,)),
                dma((4,)), dma((4,)), dma((2,)), dma((2,)),
                dma((max(n_tp - 1, 1), 6)), dma((max(n_tp - 1, 1), 6)),
                dma((peers,)), dma((peers,)),
                dma, dma,
                dma((2, 2, hmax)), dma((2, 2, hmax)),
                dma((nz,)), dma((nz,)),
                dma((nz,)), dma((nz,)), dma((nz,)), dma((nz,)),
                dma((ny,)), dma((ny,)), dma((ny,)), dma((ny,)),
                dma((nz,)), dma((nz,)), dma((nz,)), dma((nz,)),
                dma((ny,)), dma((ny,)),
                dma((max(n_tp - 1, 1), pieces)), dma((max(n_tp - 1, 1), pieces)),
            ],
            compiler_params=pltpu.CompilerParams(
                collective_id=0, has_side_effects=True, vmem_limit_bytes=56 * 1024 * 1024
            ),
            name="mixer",
        )(
            tokens, in_gain[None], wq.T, wk.T, wvv.T, wrq.T, wrf.T, wri.T, lam[None], lower, scale[None],
            att_gain[None], rec_gain[None], aow, row_w,
        )
        half = width // 2
        return pl.pallas_call(
            finish,
            grid=(2,),
            out_shape=(
                jax.ShapeDtypeStruct((rows, width), BF),
                jax.ShapeDtypeStruct((heads, rows), F32),
            ),
            in_specs=[
                pl.BlockSpec((n_tp, rows, half), lambda n: (0, 0, n)),
                pl.BlockSpec((heads, rows), lambda n: (0, 0)),
            ],
            out_specs=(
                pl.BlockSpec((rows, half), lambda n: (0, n)),
                pl.BlockSpec((heads, rows), lambda n: (0, 0)),
            ),
            name="finish",
        )(parts, lse)

    col = P(None, ("tp", "fs"))
    return jax.shard_map(
        on_device,
        mesh=mesh,
        in_specs=(
            P(("fs", "sp"), None), P(), col, col, col, col, col, col,
            P("tp"), P("tp", None), P(("fs", "sp")), P(), P(), P("tp", None), P("tp", None),
        ),
        out_specs=(P(("fs", "sp"), None), P("tp", ("fs", "sp"))),
        check_vma=False,
    )
```

time: 304 us -> 81 us (0.27)
  the two profiles are of different devices: /device:TPU:505 before, /device:TPU:65 now
where the time goes in v1:
time: 81 us; the launch traced here: 80.9 us
  Pallas kernels  80.2 us (99%)
    pallas_call x1, Pallas kernels, on_device(): pl.pallas_call(functools.partial(kernel, n_sp, n_fs, n_tp), out_shape=(ja...  78.2 us
    pallas_call x1, Pallas kernels, on_device(): pl.pallas_call(finish, grid=(2,), out_shape=(jax.ShapeDtypeStruct((rows,...  1.99 us

profile of v1, /device:TPU:65, one launch (start us, length us, event | category | flops | bytes accessed | tf_op | source)
XLA Modules:
  0.0 80.9 jit_solution(14500087960777766433)
XLA Ops:
  0.6 78.2 %mixer.1 = (bf16[2,128,2048]{2,1,0:T(8,128)(2,1)}, f32[2,128]{1,0:T(2,128)}) custom-call(bf16[128,2048]{1,0:T(8,128)(2,1)} %tok.1, f32[1,2048]{1,0:T(1,128)} %bitcast.17, bf16[64,2048]{1,0:T(8,128)(2,1)} %bitcast.11, bf16[64,2048]{1,0:T(8,128)(2,1)} %bitcast.12, bf16[64,2048]{1,0:T(8,128)(2,1)} %bitcast.13, bf16[64,2048]{1,0:T(8,128)(2,1)} %bitcast.14, ...), custom_call_target="tpu_custom_call" | custom-call | tf_op jit(solution)/shard_map/mixer/pallas_call | solution.py:568
  78.9 2.0 %finish.1 = (bf16[128,2048]{1,0:T(8,128)(2,1)}, f32[2,128]{1,0:T(2,128)}) custom-call(bf16[2,128,2048]{2,1,0:T(8,128)(2,1)} %get-tuple-element.4.parts, f32[2,128]{1,0:T(2,128)} %get-tuple-element.5.lse_in), custom_call_target="tpu_custom_call" | custom-call | tf_op jit(solution)/shard_map/finish/pallas_call | solution.py:630

commit v2 on v1

v2 whole, which is shorter than its diff:
```python
import functools

import jax
import jax.numpy as jnp
from jax import lax
from jax.experimental import pallas as pl
from jax.experimental.pallas import tpu as pltpu
from jax.sharding import PartitionSpec as P

DK = 64
DV = 128
SUB = 16
EPS = 1e-06
NEG = -1e30
MESH = pl.DeviceIdType.MESH
BF = jnp.bfloat16
F32 = jnp.float32


def dot_nt(a, b):
    return lax.dot_general(a, b, (((1,), (1,)), ((), ())), preferred_element_type=jnp.float32)


def dot_nn(a, b):
    return jnp.dot(a, b, preferred_element_type=jnp.float32)


def grid_of(n_sp):
    ny = 1
    while ny * ny < n_sp:
        ny *= 2
    return n_sp // ny, ny


def kernel(
    n_sp, n_fs, n_tp,
    tok, gain_h, w0, w1, w2, w3, w4, w5, lam_h, lower_h, scale_h, att_gain_h, rec_gain_h, aow, row_w,
    parts, lse,
    tokv, gain, lam, lower, scale, att_gain, rec_gain, aov, rov, wcat, nown, near_a, near_c, far, psend, pr, kvp, q2, kvg, qb,
    osnd, orcv, stx, lsrow, prt, m_s, l_s, acc,
    smat, olocal, qdec, lsend, lrec, tl, trec, pre, tsnd, rdsnd, zrec, zrd, r3s, s_in,
    t_sem, g_sem, w_sem, o_sem, xa_r, xc_r, xf_r, x_s, xf_s, rel_s, rel_r,
    b_s, b_r, c_s, c_r, kp_s, k0_s, kp_r, kv_s, kv_r, q_s, q_r,
    os_s, os_r, sx_s, sx_r, sy_s, sy_r, r1_s, r1_r, r1t_s, r1t_r, r2_s, r2_r, r2t_s, r2t_r, r3_s, r3_r, op_s, op_r,
):
    nz, ny = grid_of(n_sp)
    hz = nz // 2
    sl_rows = DV // ny
    z, f, t = lax.axis_index("sp"), lax.axis_index("fs"), lax.axis_index("tp")
    i, j = z // ny, lax.rem(z, ny)
    mir = nz - 1 - i
    low = jnp.minimum(i, mir)
    hd = jnp.where(i < hz, 0, 1)
    rows, width = tok.shape
    half = rows // n_tp
    qr = half // 2
    hq = qr // 2
    heads = n_fs // 2
    right, left = lax.rem(f + 1, n_fs), lax.rem(f + n_fs - 1, n_fs)
    across = lax.rem(f + 2, n_fs)
    j_r, j_l = lax.rem(j + 1, ny), lax.rem(j + ny - 1, ny)

    def remote(src, dst, s, r, **dev):
        return pltpu.make_async_remote_copy(src, dst, s, r, device_id=dev, device_id_type=MESH)

    def landed(ref, sem):
        pltpu.make_async_copy(ref, ref, sem).wait()

    def sp_of(a, b):
        return a * ny + b

    tcopy = pltpu.make_async_copy(tok, tokv, t_sem)
    tcopy.start()
    scopies = [
        pltpu.make_async_copy(a, b, g_sem.at[n])
        for n, (a, b) in enumerate((
            (gain_h, gain), (lam_h, lam), (lower_h, lower), (scale_h, scale),
            (att_gain_h, att_gain), (rec_gain_h, rec_gain),
        ))
    ]
    for c in scopies:
        c.start()
    barrier = pltpu.get_barrier_semaphore()
    for d in range(1, n_fs):
        peer = lax.rem(f + d, n_fs)
        pl.semaphore_signal(barrier, inc=1, device_id={"fs": peer}, device_id_type=MESH)
        pl.semaphore_signal(
            barrier, inc=1, device_id={"fs": peer, "sp": sp_of(mir, j)}, device_id_type=MESH
        )
    for d in range(1, n_tp):
        pl.semaphore_signal(barrier, inc=1, device_id={"tp": lax.rem(t + d, n_tp)}, device_id_type=MESH)
    for d in range(1, ny):
        pl.semaphore_signal(barrier, inc=1, device_id={"sp": sp_of(i, lax.rem(j + d, ny))}, device_id_type=MESH)
    for d in range(1, nz):
        pl.semaphore_signal(barrier, inc=1, device_id={"sp": sp_of(lax.rem(i + d, nz), j)}, device_id_type=MESH)

    wcopies = [
        pltpu.make_async_copy(w, wcat.at[pl.ds(n * DK, DK)], w_sem)
        for n, w in enumerate((w1, w2, w0, w3, w4, w5))
    ]
    for c in wcopies:
        c.start()
    ocopies = [
        pltpu.make_async_copy(aow, aov, o_sem.at[0]),
        pltpu.make_async_copy(row_w, rov, o_sem.at[1]),
    ]

    blk = 32
    tcopy.wait()
    scopies[0].wait()

    @pl.loop(0, rows // blk)
    def _(n):
        sl = pl.ds(pl.multiple_of(n * blk, blk), blk)
        x = tokv[sl, :].astype(F32)
        ms = jnp.mean(x * x, axis=-1, keepdims=True)
        nown[sl, :] = (x * lax.rsqrt(ms + EPS) * gain[...]).astype(BF)

    m_s[...] = jnp.full(m_s.shape, NEG, F32)
    l_s[...] = jnp.zeros(l_s.shape, F32)
    acc[...] = jnp.zeros(acc.shape, F32)
    for k in range(1, hz):
        @pl.when(k > i)
        def _():
            for h in range(2):
                orcv[h, k] = jnp.zeros((rows, DV), BF)
    pl.semaphore_wait(barrier, 2 * (n_fs - 1) + n_tp - 1 + ny - 1 + nz - 1)

    def own_rows(at, size):
        return nown.at[pl.ds(pl.multiple_of(t * half + at, hq), size)]

    def send_a(way, n):
        return remote(
            own_rows(way * qr + n * hq, hq), near_a.at[way, t, pl.ds(n * hq, hq)],
            x_s, xa_r.at[way, n], fs=left if way else right,
        )

    def send_c(way):
        return remote(
            own_rows((1 - way) * qr, qr), near_c.at[way, t], x_s, xc_r.at[way], fs=left if way else right
        )

    def send_f(way, n):
        at = pl.ds(n * hq, hq)
        return remote(
            near_a.at[way, t, at], far.at[t, way, at], xf_s, xf_r.at[way, n], fs=left if way else right
        )

    for n in range(2):
        for way in range(2):
            send_a(way, n).start()
    for way in range(2):
        send_c(way).start()
    for c in ocopies:
        c.start()

    def relay(idx, at):
        for e in range(1, n_tp):
            remote(at, at, rel_s.at[idx], rel_r.at[idx], tp=lax.rem(t + e, n_tp)).start()

    def relayed(idx, at):
        if n_tp > 1:
            landed(at, rel_r.at[idx])

    oth = n_tp - 1 - t

    def project(x):
        return dot_nt(x.reshape(rows, width), wcat[...]).astype(BF)

    def split(x):
        return x.reshape(n_tp, 2, qr, DV)

    landed(wcat, w_sem)


    back = (f, left, right, across)
    part = lax.rem(f, 2)
    mine = f // 2 == hd
    row_to = jnp.where(mine, i, mir)

    def kv_copy(slot, a):
        return remote(
            psend.at[slot, 0, :, a], kvp.at[hd, part, :, a], kp_s if slot else k0_s, kp_r.at[hd, part, a],
            sp=sp_of(row_to, j), fs=back[slot],
        )

    def q_part(slot, a):
        return remote(psend.at[slot, 1, :, a], pr.at[f, 0, :, a], b_s, b_r, fs=back[slot])

    def r_part(slot, a):
        return remote(psend.at[slot, 2, :, a], pr.at[f, 1, :, a], c_s, c_r, fs=back[slot])

    own = project(nown[...])
    pr[f, 0] = split(own[:, DV: 2 * DV])
    pr[f, 1] = split(own[:, 2 * DV:])

    @pl.when(mine)
    def _():
        kvp[hd, part] = split(own[:, :DV])

    @pl.when(jnp.logical_not(mine))
    def _():
        psend[0, 0] = split(own[:, :DV])
        for a in range(2):
            kv_copy(0, a).start()

    def deliver(todo, rest=()):
        for slot, a in todo:
            kv_copy(slot, a).start()
        for slot, a in rest:
            q_part(slot, a).start()
        for slot, a in rest:
            r_part(slot, a).start()

    def deliver_near(x, flip, rest):
        got = project(x)
        todo = []
        for way in range(2):
            a = 1 - way if flip else way
            for c in range(n_tp):
                lo = (way * n_tp + c) * qr
                for g in range(3):
                    psend[1 + way, g, c, a] = got[lo: lo + qr, g * DV: (g + 1) * DV]
            todo.append((1 + way, a))
        deliver(todo, rest)

    for n in range(2):
        for way in range(2):
            landed(near_a.at[way, t, pl.ds(n * hq, hq)], xa_r.at[way, n])
            send_f(way, n).start()
            relay(0, near_a.at[way, t, pl.ds(n * hq, hq)])
    relayed(0, near_a.at[:, oth])
    deliver_near(near_a[...], False, [])
    for way in range(2):
        landed(near_c.at[way, t], xc_r.at[way])
        relay(2, near_c.at[way, t])
    relayed(2, near_c.at[:, oth])
    deliver_near(near_c[...], True, [(1, 0), (2, 1)])
    for n in range(2):
        for way in range(2):
            landed(far.at[t, way, pl.ds(n * hq, hq)], xf_r.at[way, n])
            relay(1, far.at[t, way, pl.ds(n * hq, hq)])
    relayed(1, far.at[oth])
    far_rows = far[...].reshape(rows, width)
    psend[3, 0] = split(dot_nt(far_rows, wcat[:DV]).astype(BF))
    deliver([(3, 0), (3, 1)])
    got = dot_nt(far_rows, wcat[DV:]).astype(BF)
    for g in range(2):
        psend[3, 1 + g] = split(got[:, g * DV: (g + 1) * DV])
    deliver([], [(3, 0), (3, 1), (1, 1), (2, 0)])

    def flat(x):
        return x.reshape(rows, DV)

    def pair(h, g, lo):
        return jnp.concatenate([flat(pr[2 * h + p, g])[:, lo: lo + DK] for p in range(2)], axis=1)

    slot_of = (hd, 1 - hd)

    def gather_kv(role):
        g = slot_of[role]
        for p in range(2):
            @pl.when((role == 1) | (2 * hd + p != f))
            def _():
                for a in range(2):
                    landed(kvp.at[g, p, :, a], kp_r.at[g, p, a])
        got = [flat(kvp[g, p]) for p in range(2)]
        kvg[g, j, :, :DV] = jnp.concatenate([x[:, :DK] for x in got], axis=1)
        kvg[g, j, :, DV:] = jnp.concatenate([x[:, DK:] for x in got], axis=1)

    right_hops = (ny // 2, ny - 1 - ny // 2)
    left_hops = (ny - 1 - ny // 2, ny // 2)

    half_k = rows // 2

    def block(role, way, d, n):
        return kvg.at[slot_of[role], lax.rem(j + (d if way else ny - d), ny), pl.ds(n * half_k, half_k)]

    def ring(role, way, d, n):
        at = block(role, way, d, n)
        return remote(at, at, kv_s, kv_r.at[role, way, d, n], sp=sp_of(i, j_l if way else j_r))

    hops = [(right_hops[g], left_hops[g]) for g in range(2)]

    taken = set()

    def step(g, d, again=False):
        if (g, d) in taken and not again:
            return
        taken.add((g, d))
        for n in range(2):
            for way in range(2):
                if 0 < d <= hops[g][way]:
                    landed(block(g, way, d, n), kv_r.at[g, way, d - 1, n])
                if d < hops[g][way]:
                    ring(g, way, d, n).start()

    gather_kv(0)
    step(0, 0)
    gather_kv(1)
    step(1, 0)

    landed(pr.at[pl.ds(0, n_fs - 1), 0], b_r)
    for h in range(heads):
        q2[h] = (pair(h, 0, 0).astype(F32) * DK ** (-0.5)).astype(BF)
    qb[i] = q2[hd]

    def q_copy(d):
        a = lax.rem(i + d, nz)
        return remote(q2.at[jnp.where(a < hz, 0, 1)], qb.at[i], q_s, q_r, sp=sp_of(a, j))

    def wanted(a):
        return (min(a, nz - 1 - a) <= i) & (i != a)

    for d in range(1, nz):
        q_copy(d).start()

    landed(pr.at[pl.ds(0, n_fs - 1), 1], c_r)

    ri_row = lax.broadcasted_iota(jnp.int32, (rows, DV), 0)
    lane = lax.broadcasted_iota(jnp.int32, (rows, DV), 1)
    sub_pos = lax.rem(ri_row, SUB)
    tri = (
        lax.broadcasted_iota(jnp.int32, (rows, rows), 0)
        >= lax.broadcasted_iota(jnp.int32, (rows, rows), 1)
    )
    trif = tri.astype(F32)
    gates = []
    for c in scopies[1:]:
        c.wait()
    sc = jnp.broadcast_to(scale[...], (DV, rows)).T
    for h in range(heads):
        rf = pair(h, 1, 0).astype(F32)
        ri = pair(h, 1, DK).astype(F32)
        lb = lower[h: h + 1, :]
        g = sc * jnp.log(lb + (1.0 - lb) * jax.nn.sigmoid(rf))
        kk = 1.0 - jnp.exp(g)
        a = jnp.dot(trif, g, preferred_element_type=F32, precision=lax.Precision.HIGHEST)
        last = a[rows - 1: rows, :]
        kd = (kk * jnp.exp(last - a)).astype(BF)
        lsend[h] = dot_nn(ri.T.astype(BF), kd).astype(BF)
        tl[h: h + 1, :] = jnp.exp(last)
        gates.append((a, kk, ri))

    def sl_of(y):
        return pl.ds(pl.multiple_of(y * sl_rows, sl_rows), sl_rows)

    def r1(d):
        y = lax.rem(j + d, ny)
        return (
            remote(lsend.at[:, sl_of(y)], lrec.at[j], r1_s, r1_r, sp=sp_of(i, y)),
            remote(tl, trec.at[j], r1t_s, r1t_r, sp=sp_of(i, y)),
        )

    lrec[j] = lsend[:, sl_of(j), :]
    trec[j] = tl[...]
    for d in range(1, ny):
        for c in r1(d):
            c.start()

    step(0, 1)
    step(1, 1)

    def local(h):
        a, kk, ri = gates[h]
        rq = pair(h, 0, DK).astype(F32)
        qdec[h] = (rq * jnp.exp(a)).astype(BF)
        smat[h, 0:SUB, :] = jnp.zeros((SUB, rows), BF)
        for n in range(1, rows // SUB):
            lo = n * SUB
            ref = a[lo - 1: lo, :]
            qd = (rq[lo: lo + SUB] * jnp.exp(a[lo: lo + SUB] - ref)).astype(BF)
            kd = (kk * jnp.exp(jnp.where(ri_row < lo, ref - a, NEG))).astype(BF)
            smat[h, lo: lo + SUB, :] = dot_nt(qd, kd).astype(BF)
        o = dot_nn(smat[h], ri.astype(BF))
        o = o + jnp.sum(rq * kk, axis=-1, keepdims=True) * ri
        for d in range(1, SUB):
            valid = sub_pos >= d
            dec = jnp.exp(jnp.where(valid, a - pltpu.roll(a, d, 0), NEG))
            col = jnp.sum(rq * dec * pltpu.roll(kk, d, 0), axis=-1, keepdims=True)
            o = o + col * pltpu.roll(ri, d, 0)
        olocal[h] = o

    local(0)
    local(1)
    diag = (
        lax.broadcasted_iota(jnp.int32, (rows, rows), 1)
        - lax.broadcasted_iota(jnp.int32, (rows, rows), 0)
    )

    def strip(chunk, blocks, groups, offs):
        kts, vts, masks = [], [], []
        for g, masked in groups:
            for o in offs:
                y = lax.rem(j + o, ny)
                kts.append(kvg[g, y, :, :DV])
                vts.append(kvg[g, y, :, DV:])
                masks.append(diag <= (j - y) * rows if masked else None)
        kt = jnp.concatenate(kts, axis=0)
        vt = jnp.concatenate(vts, axis=0)
        scores = []
        for b in blocks:
            q = qb[b]
            for m in range(2):
                scores.append(dot_nt(jnp.where((lane < DK) if m == 0 else (lane >= DK), q, jnp.zeros_like(q)), kt))
        done = []
        for sco in scores:
            if any(x is not None for x in masks):
                sco = jnp.concatenate([
                    sco[:, n * rows: (n + 1) * rows] if x is None
                    else jnp.where(x, sco[:, n * rows: (n + 1) * rows], NEG)
                    for n, x in enumerate(masks)
                ], axis=1)
            top = jnp.max(sco, axis=-1, keepdims=True)
            e = jnp.exp(sco - top)
            done.append((top, jnp.sum(e, axis=-1, keepdims=True), dot_nn(e.astype(BF), vt)))
        for n, (top, tot, num) in enumerate(done):
            b, m = blocks[n // 2], n % 2
            m_s[chunk, b, m] = top
            l_s[chunk, b, m] = tot
            acc[chunk, b, m] = num

    high = nz - 1 - low

    def sweep(chunk, dists, between=None):
        offs = sorted({o % ny for d in dists for o in (d, -d) if d <= ny // 2})
        if not offs:
            return

        strip(chunk, [low], [(0, True)], offs)

        @pl.loop(0, (high - low - 1) // 2)
        def _(n):
            strip(chunk, [low + 1 + 2 * n, low + 2 + 2 * n], [(0, False)], offs)

        if between is not None:
            pl.when(low < hz // 2)(between)
        strip(chunk, [high], [(0, False), (1, True)], offs)
        if between is not None:
            pl.when(low >= hz // 2)(between)

        @pl.loop(high + 1, nz)
        def _(b):
            strip(chunk, [b], [(0, False), (1, False)], offs)

    step(0, 2)
    step(1, 2)

    landed(lrec.at[pl.ds(0, ny - 1)], r1_r)
    landed(trec.at[pl.ds(0, ny - 1)], r1t_r)
    run = jnp.zeros((heads, sl_rows, DV), F32)
    rd = jnp.ones((heads, DV), F32)
    for y in range(ny):
        pre[y] = run
        run = trec[y][:, None, :] * run + lrec[y].astype(F32)
        rd = rd * trec[y]
    tsnd[...] = run.astype(BF)
    rdsnd[...] = rd

    def r2(d):
        to = sp_of(lax.rem(i + d, nz), j)
        return (
            remote(tsnd, zrec.at[i], r2_s, r2_r, sp=to),
            remote(rdsnd, zrd.at[i], r2t_s, r2t_r, sp=to),
        )

    for d in range(1, nz):
        for c in r2(d):
            c.start()

    landed(qb.at[pl.ds(0, nz - 1)], q_r)

    def row_of(h, k):
        return jnp.where(h == 0, k, nz - 1 - k)

    def stat_copy(chunk, d):
        at = stx.at[hd, low, chunk]
        return remote(at, at, sx_s.at[chunk], sx_r.at[chunk], sp=sp_of(row_of(hd, lax.rem(low + d, hz)), j))

    def emit(chunk):
        st = jnp.zeros((rows, DV), F32)
        for b in range(nz):
            for m in range(2):
                st = jnp.where(lane == m * nz + b, m_s[chunk, b, m], st)
                st = jnp.where(lane == (2 + m) * nz + b, l_s[chunk, b, m], st)
        stx[hd, low, chunk] = st.T[:4 * nz, :]
        for d in range(1, hz):
            stat_copy(chunk, d).start()

    def lse_copy(k):
        b = row_of(1 - hd, k)
        return remote(
            lsrow.at[hd, pl.ds(b, 1)], lsrow.at[hd, pl.ds(b, 1)], sy_s, sy_r, sp=sp_of(b, j)
        )

    def out_copy(b):
        return remote(osnd.at[b], orcv.at[hd, low], os_s.at[b], os_r.at[hd, low], sp=sp_of(b, j))

    def third():
        for g in range(2):
            step(g, 3, True)

    sweep(0, (0, 1, 2), between=third)
    emit(0)
    for d in range(3, ny // 2 + 1):
        for g in range(2):
            step(g, d)

    landed(zrec.at[pl.ds(0, nz - 1)], r2_r)
    landed(zrd.at[pl.ds(0, nz - 1)], r2t_r)
    run = jnp.zeros((heads, sl_rows, DV), F32)
    for a in range(nz - 1):
        run = jnp.where(a < i, zrd[a][:, None, :] * run + zrec[a].astype(F32), run)
    for y in range(ny):
        r3s[y] = (run + pre[y]).astype(BF)
        run = trec[y][:, None, :] * run

    def r3(d):
        y = lax.rem(j + d, ny)
        return remote(r3s.at[y], s_in.at[:, sl_of(j)], r3_s, r3_r, sp=sp_of(i, y))

    s_in[:, sl_of(j), :] = r3s[j]
    for d in range(1, ny):
        r3(d).start()

    sweep(1, range(3, ny // 2 + 1))
    emit(1)

    lam_h = jnp.where(hd == 0, lam[0, 0], lam[0, 1])

    def send_out(b, num):
        @pl.when(b == i)
        def _():
            orcv[hd, low] = num

        @pl.when(b != i)
        def _():
            osnd[b] = num
            out_copy(b).start()

    @pl.when(low == 0)
    def _():
        weights = []
        for m in range(2):
            tops = [stx[hd, 0, chunk, m * nz: m * nz + 1, :] for chunk in range(2)]
            tots = [stx[hd, 0, chunk, (2 + m) * nz: (2 + m) * nz + 1, :] for chunk in range(2)]
            top = jnp.maximum(tops[0], tops[1])
            scales = [jnp.exp(x - top) for x in tops]
            total = scales[0] * tots[0] + scales[1] * tots[1]
            for x in scales:
                weights.append(-lam_h * (x / total) if m else x / total)
        wt = jnp.concatenate(weights + [jnp.zeros((DV - 4, DV), F32)], axis=0).T
        num = jnp.zeros((rows, DV), F32)
        for m in range(2):
            for chunk in range(2):
                at = 2 * m + chunk
                num = num + acc[chunk, 0, m] * wt[:, at: at + 1]
        send_out(0, num.astype(BF))

    landed(r3s.at[pl.ds(0, ny - 1)], r3_r)
    recs = []
    rg = rec_gain[...]
    for h in range(heads):
        o = olocal[h] + dot_nt(qdec[h], s_in[h])
        ms = jnp.mean(o * o, axis=-1, keepdims=True)
        recs.append((o * lax.rsqrt(ms + EPS) * rg).astype(BF))
    rec = jnp.concatenate(recs, axis=1)
    for c in ocopies:
        c.wait()
    pieces = 4
    cols = width // pieces
    for n in range(pieces):
        sl = slice(n * cols, (n + 1) * cols)
        prt[:, sl] = dot_nn(rec, rov[:, sl])

    if hz > 1:
        for chunk in range(2):
            landed(stx.at[0, pl.ds(0, hz - 1), chunk], sx_r.at[chunk])

    def stat(k, chunk, r):
        return stx[hd, k, chunk, r * nz: (r + 1) * nz, :]

    sources = [(k, chunk) for k in range(hz) for chunk in range(2)]
    weights = []
    for m in range(2):
        top = stat(0, 0, m)
        for k, chunk in sources[1:]:
            top = jnp.maximum(top, stat(k, chunk, m))
        total = jnp.zeros((nz, DV), F32)
        for k, chunk in sources:
            total = total + jnp.exp(stat(k, chunk, m) - top) * stat(k, chunk, 2 + m)
        if m == 0:
            lsrow[hd] = top + jnp.log(total)
        for chunk in range(2):
            wt = jnp.exp(stx[hd, low, chunk, pl.ds(m * nz, nz), :] - top) / total
            weights.append(-lam_h * wt if m else wt)

    @pl.when(low == 0)
    def _():
        for k in range(hz):
            lse_copy(k).start()

    wt = jnp.concatenate(weights + [jnp.zeros((DV - 4 * nz, DV), F32)], axis=0).T
    for b in range(1, nz):
        @pl.when(b >= low)
        def _():
            num = jnp.zeros((rows, DV), F32)
            for m in range(2):
                for chunk in range(2):
                    at = (2 * m + chunk) * nz + b
                    num = num + acc[chunk, b, m] * wt[:, at: at + 1]
            send_out(b, num.astype(BF))

    landed(lsrow.at[0, pl.ds(0, 1)], sy_r)
    for k in range(hz):
        for h in range(2):
            @pl.when((k <= i) & ((hd != h) | (low != k)))
            def _():
                landed(orcv.at[h, k], os_r.at[h, k])

    atts = []
    ag = att_gain[...]
    for h in range(heads):
        lse[h: h + 1, :] = lsrow[h, pl.ds(i, 1), :]
        x = orcv[h, 0].astype(F32)
        for k in range(1, hz):
            x = x + orcv[h, k].astype(F32)
        ms = jnp.mean(x * x, axis=-1, keepdims=True)
        atts.append((x * lax.rsqrt(ms + EPS) * ag * 0.8).astype(BF))
    att = jnp.concatenate(atts, axis=1)

    for n in range(pieces):
        sl = slice(n * cols, (n + 1) * cols)
        parts[0, :, sl] = (dot_nn(att, aov[:, sl]) + prt[:, sl]).astype(BF)
        for e in range(1, n_tp):
            c = remote(
                parts.at[0, :, sl], parts.at[e, :, sl], op_s, op_r,
                tp=lax.rem(t + e, n_tp),
            )
            c.start()

    landed(nown, x_s)
    landed(near_a.at[:, 0], xf_s)
    if n_tp > 1:
        landed(near_a.at[:, 0], rel_s.at[0])
        landed(far.at[0], rel_s.at[1])
        landed(near_c.at[:, 0], rel_s.at[2])
    landed(psend.at[pl.ds(1, n_fs - 1), 0], kp_s)
    landed(psend.at[pl.ds(1, n_fs - 1), 1], b_s)
    landed(psend.at[pl.ds(1, n_fs - 1), 2], c_s)

    @pl.when(jnp.logical_not(mine))
    def _():
        landed(psend.at[0, 0], k0_s)

    landed(kvg.at[:, pl.ds(0, ny - 1)], kv_s)
    landed(qb.at[pl.ds(0, nz - 1)], q_s)
    landed(lrec.at[pl.ds(0, ny - 1)], r1_s)
    landed(trec.at[pl.ds(0, ny - 1)], r1t_s)
    landed(zrec.at[pl.ds(0, nz - 1)], r2_s)
    landed(zrd.at[pl.ds(0, nz - 1)], r2t_s)
    landed(r3s.at[pl.ds(0, ny - 1)], r3_s)
    if hz > 1:
        for chunk in range(2):
            landed(stx.at[0, pl.ds(0, hz - 1), chunk], sx_s.at[chunk])

    @pl.when(low == 0)
    def _():
        landed(lsrow.at[0, pl.ds(0, hz)], sy_s)

    for a in range(nz):
        @pl.when((a >= low) & (i != a))
        def _():
            out_copy(a).wait_send()
    if n_tp > 1:
        landed(parts.at[0], op_s)
        landed(parts.at[1], op_r)


def finish(parts, lse_in, mixed, lse):
    total = parts[0].astype(jnp.float32)
    for e in range(1, parts.shape[0]):
        total = total + parts[e].astype(jnp.float32)
    mixed[...] = total.astype(jnp.bfloat16)
    lse[...] = lse_in[...]


def solution(mesh):
    n_sp, n_fs, n_tp = (mesh.shape[k] for k in ("sp", "fs", "tp"))
    nz, ny = grid_of(n_sp)

    def on_device(
        tokens, in_gain, wq, wk, wvv, wrq, wrf, wri, lam, lower, scale, att_gain, rec_gain, aow, row_w
    ):
        rows, width = tokens.shape
        heads = lower.shape[0]
        assert heads == 2 and n_fs == 4 and rows == DV and nz % 2 == 0
        vm = pl.BlockSpec(memory_space=pltpu.VMEM)
        hbm = pl.BlockSpec(memory_space=pltpu.HBM)
        dma = pltpu.SemaphoreType.DMA
        qr = rows // (2 * n_tp)
        slr = DV // ny
        hmax = max(ny // 2, 1)
        parts, lse = pl.pallas_call(
            functools.partial(kernel, n_sp, n_fs, n_tp),
            out_shape=(pltpu.VMEM((n_tp, rows, width), BF), pltpu.VMEM((heads, rows), F32)),
            in_specs=[hbm] * 15,
            out_specs=(vm, vm),
            scratch_shapes=[
                pltpu.VMEM(tokens.shape, BF),
                pltpu.VMEM((1, width), F32),
                pltpu.SMEM((1, heads), F32),
                pltpu.VMEM((heads, DV), F32),
                pltpu.VMEM((1, rows), F32),
                pltpu.VMEM((1, DV), F32),
                pltpu.VMEM((1, DV), F32),
                pltpu.VMEM(aow.shape, BF),
                pltpu.VMEM(row_w.shape, BF),
                pltpu.VMEM((6 * DK, width), BF),
                pltpu.VMEM((rows, width), BF),
                pltpu.VMEM((2, n_tp, qr, width), BF),
                pltpu.VMEM((2, n_tp, qr, width), BF),
                pltpu.VMEM((n_tp, 2, qr, width), BF),
                pltpu.VMEM((n_fs, 3, n_tp, 2, qr, DV), BF),
                pltpu.VMEM((n_fs, 2, n_tp, 2, qr, DV), BF),
                pltpu.VMEM((2, 2, n_tp, 2, qr, DV), BF),
                pltpu.VMEM((heads, rows, DV), BF),
                pltpu.VMEM((2, ny, rows, 2 * DV), BF),
                pltpu.VMEM((nz, rows, DV), BF),
                pltpu.VMEM((nz, rows, DV), BF),
                pltpu.VMEM((2, nz // 2, rows, DV), BF),
                pltpu.VMEM((2, nz // 2, 2, 4 * nz, DV), F32),
                pltpu.VMEM((2, nz, DV), F32),
                pltpu.VMEM((rows, width), F32),
                pltpu.VMEM((2, nz, 2, rows, 1), F32),
                pltpu.VMEM((2, nz, 2, rows, 1), F32),
                pltpu.VMEM((2, nz, 2, rows, DV), F32),
                pltpu.VMEM((heads, rows, rows), BF),
                pltpu.VMEM((heads, rows, DV), F32),
                pltpu.VMEM((heads, rows, DV), BF),
                pltpu.VMEM((heads, DV, DV), BF),
                pltpu.VMEM((ny, heads, slr, DV), BF),
                pltpu.VMEM((heads, DV), F32),
                pltpu.VMEM((ny, heads, DV), F32),
                pltpu.VMEM((ny, heads, slr, DV), F32),
                pltpu.VMEM((heads, slr, DV), BF),
                pltpu.VMEM((heads, DV), F32),
                pltpu.VMEM((nz, heads, slr, DV), BF),
                pltpu.VMEM((nz, heads, DV), F32),
                pltpu.VMEM((ny, heads, slr, DV), BF),
                pltpu.VMEM((heads, DV, DV), BF),
                dma, dma((6,)), dma, dma((2,)),
                dma((2, 2)), dma((2,)), dma((2, 2)), dma, dma, dma((3,)), dma((3,)),
                dma, dma, dma, dma, dma, dma, dma((2, 2, 2)),
                dma, dma((2, 2, hmax, 2)), dma, dma,
                dma((nz,)), dma((2, nz // 2)), dma((2,)), dma((2,)), dma, dma,
                dma, dma, dma, dma, dma, dma, dma, dma, dma, dma,
                dma, dma,
            ],
            compiler_params=pltpu.CompilerParams(
                collective_id=0, has_side_effects=True, vmem_limit_bytes=56 * 1024 * 1024
            ),
            name="mixer",
        )(
            tokens, in_gain[None], wq.T, wk.T, wvv.T, wrq.T, wrf.T, wri.T, lam[None], lower, scale[None],
            att_gain[None], rec_gain[None], aow, row_w,
        )
        return pl.pallas_call(
            finish,
            out_shape=(
                jax.ShapeDtypeStruct((rows, width), BF),
                jax.ShapeDtypeStruct((heads, rows), F32),
            ),
            in_specs=[vm, vm],
            out_specs=(vm, vm),
            compiler_params=pltpu.CompilerParams(vmem_limit_bytes=8 * 1024 * 1024),
            name="finish",
        )(parts, lse)

    col = P(None, ("tp", "fs"))
    return jax.shard_map(
        on_device,
        mesh=mesh,
        in_specs=(
            P(("fs", "sp"), None), P(), col, col, col, col, col, col,
            P("tp"), P("tp", None), P(("fs", "sp")), P(), P(), P("tp", None), P("tp", None),
        ),
        out_specs=(P(("fs", "sp"), None), P("tp", ("fs", "sp"))),
        check_vma=False,
    )
```

time: 81 us -> 62.9 us (0.78)
  the two profiles are of different devices: /device:TPU:65 before, /device:TPU:1 now
where the time goes in v2:
time: 62.9 us; the launch traced here: 62.6 us
  Pallas kernels  61.9 us (98%)
  between operations  0.64 us (1%)
    pallas_call x1, Pallas kernels, on_device(): pl.pallas_call(functools.partial(kernel, n_sp, n_fs, n_tp), out_shape=(pl...  61 us

profile of v2, /device:TPU:1, one launch (start us, length us, event | category | flops | bytes accessed | tf_op | source)
XLA Modules:
  0.0 62.6 jit_solution(9375062707454137034)
XLA Ops:
  0.6 61.0 %mixer.1 = (bf16[2,128,2048]{2,1,0:T(8,128)(2,1)S(1)}, f32[2,128]{1,0:T(2,128)S(1)}) custom-call(bf16[128,2048]{1,0:T(8,128)(2,1)} %tok.1, f32[1,2048]{1,0:T(1,128)} %bitcast.17, bf16[64,2048]{1,0:T(8,128)(2,1)} %bitcast.11, bf16[64,2048]{1,0:T(8,128)(2,1)} %bitcast.12, bf16[64,2048]{1,0:T(8,128)(2,1)} %bitcast.13, bf16[64,2048]{1,0:T(8,128)(2,1)} %bitcast.14, ...), custom_call_target="tpu_custom_call" | custom-call | tf_op jit(solution)/shard_map/mixer/pallas_call | solution.py:704
  61.7 0.9 %finish.1 = (bf16[128,2048]{1,0:T(8,128)(2,1)}, f32[2,128]{1,0:T(2,128)}) custom-call(bf16[2,128,2048]{2,1,0:T(8,128)(2,1)S(1)} %get-tuple-element.4.parts, f32[2,128]{1,0:T(2,128)S(1)} %get-tuple-element.5.lse_in), custom_call_target="tpu_custom_call" | custom-call | tf_op jit(solution)/shard_map/finish/pallas_call | solution.py:768

commit v3 on v2

--- a/solution.py
+++ b/solution.py
@@ -39,7 +39,7 @@
     tokv, gain, lam, lower, scale, att_gain, rec_gain, aov, rov, wcat, nown, near_a, near_c, far, psend, pr, kvp, q2, kvg, qb,
     osnd, orcv, stx, lsrow, prt, m_s, l_s, acc,
     smat, olocal, qdec, lsend, lrec, tl, trec, pre, tsnd, rdsnd, zrec, zrd, r3s, s_in,
-    t_sem, g_sem, w_sem, o_sem, xa_r, xc_r, xf_r, x_s, xf_s, rel_s, rel_r,
+    t_sem, g_sem, w_sem, wx_s, wx_r, o_sem, xa_r, xc_r, xf_r, x_s, xf_s, rel_s, rel_r,
     b_s, b_r, c_s, c_r, kp_s, k0_s, kp_r, kv_s, kv_r, q_s, q_r,
     os_s, os_r, sx_s, sx_r, sy_s, sy_r, r1_s, r1_r, r1t_s, r1t_r, r2_s, r2_r, r2t_s, r2t_r, r3_s, r3_r, op_s, op_r,
 ):
@@ -81,6 +81,11 @@
     for c in scopies:
         c.start()
     barrier = pltpu.get_barrier_semaphore()
+    oth = n_tp - 1 - t
+    for row in (i, mir):
+        pl.semaphore_signal(
+            barrier, inc=1, device_id={"fs": across, "sp": sp_of(row, j), "tp": oth}, device_id_type=MESH
+        )
     for d in range(1, n_fs):
         peer = lax.rem(f + d, n_fs)
         pl.semaphore_signal(barrier, inc=1, device_id={"fs": peer}, device_id_type=MESH)
@@ -95,7 +100,7 @@
         pl.semaphore_signal(barrier, inc=1, device_id={"sp": sp_of(lax.rem(i + d, nz), j)}, device_id_type=MESH)
 
     wcopies = [
-        pltpu.make_async_copy(w, wcat.at[pl.ds(n * DK, DK)], w_sem)
+        pltpu.make_async_copy(w, wcat.at[pl.ds(DV + n * DK, DK)], w_sem)
         for n, w in enumerate((w1, w2, w0, w3, w4, w5))
     ]
     for c in wcopies:
@@ -124,7 +129,7 @@
         def _():
             for h in range(2):
                 orcv[h, k] = jnp.zeros((rows, DV), BF)
-    pl.semaphore_wait(barrier, 2 * (n_fs - 1) + n_tp - 1 + ny - 1 + nz - 1)
+    pl.semaphore_wait(barrier, 2 + 2 * (n_fs - 1) + n_tp - 1 + ny - 1 + nz - 1)
 
     def own_rows(at, size):
         return nown.at[pl.ds(pl.multiple_of(t * half + at, hq), size)]
@@ -162,15 +167,15 @@
         if n_tp > 1:
             landed(at, rel_r.at[idx])
 
-    oth = n_tp - 1 - t
-
     def project(x):
-        return dot_nt(x.reshape(rows, width), wcat[...]).astype(BF)
+        return dot_nt(x.reshape(rows, width), wcat[DV:]).astype(BF)
 
     def split(x):
         return x.reshape(n_tp, 2, qr, DV)
 
-    landed(wcat, w_sem)
+    landed(wcat.at[pl.ds(DV, 6 * DK)], w_sem)
+    wx = remote(wcat.at[pl.ds(DV, DV)], wcat.at[pl.ds(0, DV)], wx_s, wx_r, tp=oth)
+    wx.start()
 
 
     back = (f, left, right, across)
@@ -240,11 +245,18 @@
         for way in range(2):
             landed(far.at[t, way, pl.ds(n * hq, hq)], xf_r.at[way, n])
             relay(1, far.at[t, way, pl.ds(n * hq, hq)])
+    wx.wait_recv()
+    got = dot_nt(far[t].reshape(half, width), wcat[: 2 * DV]).astype(BF)
+    psend[3, 0, 0] = got[:, DV:].reshape(2, qr, DV)
+    psend[3, 0, 1] = got[:, :DV].reshape(2, qr, DV)
+    for n, core in enumerate((t, oth)):
+        remote(
+            psend.at[3, 0, n], kvp.at[hd, part, t], kp_s, kp_r.at[hd, part, t],
+            sp=sp_of(row_to, j), fs=across, tp=core,
+        ).start()
     relayed(1, far.at[oth])
     far_rows = far[...].reshape(rows, width)
-    psend[3, 0] = split(dot_nt(far_rows, wcat[:DV]).astype(BF))
-    deliver([(3, 0), (3, 1)])
-    got = dot_nt(far_rows, wcat[DV:]).astype(BF)
+    got = dot_nt(far_rows, wcat[2 * DV:]).astype(BF)
     for g in range(2):
         psend[3, 1 + g] = split(got[:, g * DV: (g + 1) * DV])
     deliver([], [(3, 0), (3, 1), (1, 1), (2, 0)])
@@ -640,6 +652,7 @@
             c.start()
 
     landed(nown, x_s)
+    wx.wait_send()
     landed(near_a.at[:, 0], xf_s)
     if n_tp > 1:
         landed(near_a.at[:, 0], rel_s.at[0])
@@ -694,7 +707,7 @@
     ):
         rows, width = tokens.shape
         heads = lower.shape[0]
-        assert heads == 2 and n_fs == 4 and rows == DV and nz % 2 == 0
+        assert heads == 2 and n_fs == 4 and n_tp == 2 and rows == DV and nz % 2 == 0
         vm = pl.BlockSpec(memory_space=pltpu.VMEM)
         hbm = pl.BlockSpec(memory_space=pltpu.HBM)
         dma = pltpu.SemaphoreType.DMA
@@ -716,7 +729,7 @@
                 pltpu.VMEM((1, DV), F32),
                 pltpu.VMEM(aow.shape, BF),
                 pltpu.VMEM(row_w.shape, BF),
-                pltpu.VMEM((6 * DK, width), BF),
+                pltpu.VMEM((DV + 6 * DK, width), BF),
                 pltpu.VMEM((rows, width), BF),
                 pltpu.VMEM((2, n_tp, qr, width), BF),
                 pltpu.VMEM((2, n_tp, qr, width), BF),
@@ -749,7 +762,7 @@
                 pltpu.VMEM((nz, heads, DV), F32),
                 pltpu.VMEM((ny, heads, slr, DV), BF),
                 pltpu.VMEM((heads, DV, DV), BF),
-                dma, dma((6,)), dma, dma((2,)),
+                dma, dma((6,)), dma, dma, dma, dma((2,)),
                 dma((2, 2)), dma((2,)), dma((2, 2)), dma, dma, dma((3,)), dma((3,)),
                 dma, dma, dma, dma, dma, dma, dma((2, 2, 2)),
                 dma, dma((2, 2, hmax, 2)), dma, dma,

time: 62.9 us -> 62.4 us (level)
  no operation moved by 1% of the time
where the time goes in v3:
time: 62.4 us; the launch traced here: 62.3 us
  Pallas kernels  61.7 us (99%)
  between operations  0.64 us (1%)
    pallas_call x1, Pallas kernels, on_device(): pl.pallas_call(functools.partial(kernel, n_sp, n_fs, n_tp), out_shape=(pl...  60.7 us

profile of v3, /device:TPU:1, one launch (start us, length us, event | category | flops | bytes accessed | tf_op | source)
XLA Modules:
  0.0 62.3 jit_solution(6711836359816732971)
XLA Ops:
  0.6 60.7 %mixer.1 = (bf16[2,128,2048]{2,1,0:T(8,128)(2,1)S(1)}, f32[2,128]{1,0:T(2,128)S(1)}) custom-call(bf16[128,2048]{1,0:T(8,128)(2,1)} %tok.1, f32[1,2048]{1,0:T(1,128)} %bitcast.17, bf16[64,2048]{1,0:T(8,128)(2,1)} %bitcast.11, bf16[64,2048]{1,0:T(8,128)(2,1)} %bitcast.12, bf16[64,2048]{1,0:T(8,128)(2,1)} %bitcast.13, bf16[64,2048]{1,0:T(8,128)(2,1)} %bitcast.14, ...), custom_call_target="tpu_custom_call" | custom-call | tf_op jit(solution)/shard_map/mixer/pallas_call | solution.py:717
  61.4 0.9 %finish.1 = (bf16[128,2048]{1,0:T(8,128)(2,1)}, f32[2,128]{1,0:T(2,128)}) custom-call(bf16[2,128,2048]{2,1,0:T(8,128)(2,1)S(1)} %get-tuple-element.4.parts, f32[2,128]{1,0:T(2,128)S(1)} %get-tuple-element.5.lse_in), custom_call_target="tpu_custom_call" | custom-call | tf_op jit(solution)/shard_map/finish/pallas_call | solution.py:781
